TPU v7x, 32 devices: a whole 2x2x4 slice. The times are simulated.
32 devices in a mesh: sp: 16 (over z, x, core), tp: 2 (over y).
Axes of the slice: x: 2, y: 2, z: 4, core: 2. Of those that a mesh axis runs over, the one named last changes fastest.
Arguments:
- layer_cot: bfloat16 [4096, 2048], P('sp'), may hold values from -6 to 6
- moe_input: bfloat16 [4096, 2048], P('sp'), may hold values from -6 to 6
- routes: int32 [4096, 2], P('sp'), may hold values from 0 to 15, all different within a row; in each aligned block of 256 rows (0 to 255, 256 to 511, ...) at most 48 rows name the same one
- route_weights: float32 [4096, 2], P('sp'), may hold values from 0.1 to 1.2
- gate_proj: bfloat16 [16, 2048, 1024], P('sp', None, 'tp'), may hold values from -0.125 to 0.125
- up_proj: bfloat16 [16, 2048, 1024], P('sp', None, 'tp'), may hold values from -0.125 to 0.125
- down_proj: bfloat16 [16, 1024, 2048], P('sp', 'tp'), may hold values from -0.1875 to 0.1875
- out_proj: bfloat16 [2048, 2048], P('tp'), may hold values from -0.0625 to 0.0625
- mixer_out: bfloat16 [4096, 2048], P('sp', 'tp'), may hold values from -6 to 6
- queries: bfloat16 [4096, 1024], P('sp', 'tp'), may hold values from -0.75 to 0.75
- key_rows: bfloat16 [4096, 1024], P('sp', 'tp'), may hold values from -0.75 to 0.75
- values: bfloat16 [4096, 2048], P('sp', 'tp'), may hold values from -6 to 6
- log_decay: float32 [4096, 1024], P('sp', 'tp'), may hold values from -2 to 0, as said below
- saved_state: float32 [16, 32, 32, 64], P('sp', 'tp'), may hold values from -6 to 6
Outputs:
- grad_gate: bfloat16 [16, 2048, 1024], P('sp', None, 'tp')
- grad_up: bfloat16 [16, 2048, 1024], P('sp', None, 'tp')
- grad_down: bfloat16 [16, 1024, 2048], P('sp', 'tp')
- grad_outproj: float32 [2048, 2048], P('sp', 'tp')
- grad_queries: bfloat16 [4096, 1024], P('sp', 'tp')
- grad_keys: bfloat16 [4096, 1024], P('sp', 'tp')
- grad_values: bfloat16 [4096, 2048], P('sp', 'tp')
- grad_decay: float32 [4096, 1024], P('sp', 'tp')
Inputs may be any that keep to these rules, and one draw needn't show every extreme that they name: `routes`: each row names 2 different experts; no expert is named by more than 48 of the tokens of one index of sp, and in every draw some expert is named exactly 48 times by one such span. `log_decay`: log decays are negative.
All inputs are finite; a program needn't handle non-finite values.
Results may differ from a plain program's by a relative error of at most 0.014.
Values may be sent and summed in bfloat16 or wider, within the bound.
A program may use at most 192 MiB of HBM per device.

v0:
```python
import jax
import jax.numpy as jnp
from jax import lax
from jax.sharding import PartitionSpec as P

KEY_CHANNELS = 32
DV = 64
BLOCK = 64


highest = lax.Precision.HIGHEST


def entering(part, axis, combine, identity):
    count = lax.axis_size(axis)
    place = lax.axis_index(axis)
    ahead = count - 1 - place
    gathered = jax.tree.map(lambda a: lax.all_gather(a, axis), part)
    state = jax.tree.map(lambda a, e: jnp.zeros_like(a) + jnp.asarray(e, a.dtype), part, identity)

    def one(step, state):
        source = count - 1 - step
        return combine(
            state, jax.tree.map(lambda a: lax.dynamic_index_in_dim(a, source, 0, False), gathered)
        )

    return lax.fori_loop(0, ahead, one, state)


def to_blocks(tensor, col_width):
    block_count = tensor.shape[0] // BLOCK
    head_count = tensor.shape[1] // col_width
    return (
        tensor.astype(jnp.float32)
        .reshape(block_count, BLOCK, head_count, col_width)
        .transpose(0, 2, 1, 3)
    )


def from_blocks(tensor):
    block_count, head_count, length, col_width = tensor.shape
    return tensor.transpose(0, 2, 1, 3).reshape(block_count * length, head_count * col_width)


def block_grads(queries, key_rows, values, cumulative, out_grad, state_in, from_later):
    final_log = cumulative[:, -1, :]
    token_positions = jnp.arange(cumulative.shape[1], dtype=jnp.int32)
    causal_mask = (token_positions[:, None] >= token_positions[None, :])[None, :, :, None]
    log_gaps = cumulative[:, :, None, :] - cumulative[:, None, :, :]
    decays = jnp.where(causal_mask, jnp.exp(jnp.where(causal_mask, log_gaps, 0.0)), 0.0)
    scores = jnp.einsum("htd,hsd,htsd->hts", queries, key_rows, decays, precision=highest)
    couplings = jnp.einsum("htv,hsv->hts", out_grad, values, precision=highest)
    to_end = jnp.exp(final_log[:, None, :] - cumulative)
    grad_queries = jnp.exp(cumulative) * jnp.einsum(
        "hdv,htv->htd", state_in, out_grad, precision=highest
    ) + jnp.einsum("hts,hsd,htsd->htd", couplings, key_rows, decays, precision=highest)
    grad_keys = to_end * jnp.einsum(
        "hdv,hsv->hsd", from_later, values, precision=highest
    ) + jnp.einsum("hts,htd,htsd->hsd", couplings, queries, decays, precision=highest)
    grad_values = jnp.einsum(
        "hdv,hsd->hsv", from_later, key_rows * to_end, precision=highest
    ) + jnp.einsum("hts,htv->hsv", scores, out_grad, precision=highest)
    grad_cumul = queries * grad_queries - key_rows * grad_keys
    to_start = jnp.exp(final_log)[:, :, None] * from_later + jnp.einsum(
        "htd,htv->hdv", queries * jnp.exp(cumulative), out_grad, precision=highest
    )
    return (to_start, (grad_queries, grad_keys, grad_values, grad_cumul))


def dispatch_table(routes, experts, capacity):
    flat_routes = routes.reshape(-1)
    assign_count = flat_routes.shape[0]
    onehot = (flat_routes[:, None] == jnp.arange(experts, dtype=jnp.int32)[None, :]).astype(
        jnp.int32
    )
    before = jnp.cumsum(onehot, axis=0) - onehot
    slot_ranks = jnp.sum(before * onehot, axis=1)
    places = flat_routes * capacity + slot_ranks
    sources = (
        jnp.full((experts * capacity,), assign_count, jnp.int32)
        .at[places]
        .set(jnp.arange(assign_count, dtype=jnp.int32))
    )
    return (places, sources)


def build_rows(columns_in, columns_cot, sources, route_weights, top_count, experts, capacity):
    assign_count = route_weights.shape[0] * route_weights.shape[1]
    filled = sources < assign_count
    clipped = jnp.minimum(sources, assign_count - 1)
    token_ids = clipped // top_count
    slot_weights = jnp.where(filled, route_weights.reshape(-1)[clipped], 0.0)
    rows_in = jnp.where(
        filled[:, None], jnp.take(columns_in, token_ids, axis=0), jnp.zeros((), columns_in.dtype)
    )
    rows_cot = (
        slot_weights[:, None] * jnp.take(columns_cot, token_ids, axis=0).astype(jnp.float32)
    ).astype(jnp.bfloat16)
    col_width = columns_in.shape[1]
    return (
        rows_in.reshape(experts, capacity, col_width),
        rows_cot.reshape(experts, capacity, col_width),
    )


def combine_back(returned, places, cot_columns, top_count):
    col_width = returned.shape[2]
    picked = jnp.take(returned.reshape(-1, col_width), places, axis=0).astype(jnp.float32)
    moe_grad = jnp.sum(picked.reshape(-1, top_count, col_width), axis=1)
    return (cot_columns.astype(jnp.float32) + moe_grad).astype(jnp.bfloat16)


def body(
    layer_cot,
    moe_input,
    routes,
    route_weights,
    gate_proj,
    up_proj,
    down_proj,
    out_proj,
    mixer_out,
    queries,
    key_rows,
    values,
    log_decay,
    saved_state,
):
    sp_count = lax.axis_size("sp")
    tp_count = lax.axis_size("tp")
    local_experts = gate_proj.shape[0]
    experts = local_experts * sp_count
    tok_local, model_width = layer_cot.shape
    top_count = routes.shape[1]
    capacity = 3 * tok_local // experts
    quarter = model_width // tp_count
    tp_rank = lax.axis_index("tp")
    places, sources = dispatch_table(routes, experts, capacity)
    part_in = lax.dynamic_slice_in_dim(moe_input, tp_rank * quarter, quarter, 1)
    part_cot = lax.dynamic_slice_in_dim(layer_cot, tp_rank * quarter, quarter, 1)
    rows_in, rows_cot = build_rows(
        part_in, part_cot, sources, route_weights, top_count, experts, capacity
    )
    got_in, got_cot = (
        lax.all_to_all(rows_in, "sp", split_axis=0, concat_axis=1, tiled=True),
        lax.all_to_all(rows_cot, "sp", split_axis=0, concat_axis=1, tiled=True),
    )
    got_in, got_cot = (
        lax.all_gather(got_in, "tp", axis=2, tiled=True),
        lax.all_gather(got_cot, "tp", axis=2, tiled=True),
    )
    pre_gate = jnp.einsum("erd,edf->erf", got_in, gate_proj, preferred_element_type=jnp.float32)
    pre_up = jnp.einsum("erd,edf->erf", got_in, up_proj, preferred_element_type=jnp.float32)
    sigmoid_gate = jax.nn.sigmoid(pre_gate)
    hidden = (pre_gate * sigmoid_gate * pre_up).astype(jnp.bfloat16)
    grad_hidden = jnp.einsum("erd,efd->erf", got_cot, down_proj, preferred_element_type=jnp.float32)
    grad_down = jnp.einsum(
        "erf,erd->efd", hidden, got_cot, preferred_element_type=jnp.float32
    ).astype(jnp.bfloat16)
    grad_pre_gate = (
        grad_hidden * pre_up * sigmoid_gate * (1.0 + pre_gate * (1.0 - sigmoid_gate))
    ).astype(jnp.bfloat16)
    grad_pre_up = (grad_hidden * pre_gate * sigmoid_gate).astype(jnp.bfloat16)
    grad_gate = jnp.einsum(
        "erd,erf->edf", got_in, grad_pre_gate, preferred_element_type=jnp.float32
    ).astype(jnp.bfloat16)
    grad_up = jnp.einsum(
        "erd,erf->edf", got_in, grad_pre_up, preferred_element_type=jnp.float32
    ).astype(jnp.bfloat16)
    partial_value = jnp.einsum(
        "erf,edf->erd", grad_pre_gate, gate_proj, preferred_element_type=jnp.float32
    ) + jnp.einsum("erf,edf->erd", grad_pre_up, up_proj, preferred_element_type=jnp.float32)
    summed = lax.psum_scatter(
        partial_value.astype(jnp.bfloat16), "tp", scatter_dimension=2, tiled=True
    )
    returned = lax.all_to_all(summed, "sp", split_axis=1, concat_axis=0, tiled=True)
    cot_part = lax.dynamic_slice_in_dim(layer_cot, tp_rank * quarter, quarter, 1)
    mix_part = combine_back(returned, places, cot_part, top_count)
    mix_grad = lax.all_gather(mix_part, "tp", axis=1, tiled=True)
    out_grad = lax.dot_general(
        mix_grad, out_proj, (((1,), (1,)), ((), ())), preferred_element_type=jnp.float32
    ).astype(jnp.bfloat16)
    grad_outproj = lax.psum_scatter(
        lax.dot_general(
            mix_grad, mixer_out, (((0,), (0,)), ((), ())), preferred_element_type=jnp.float32
        ),
        "sp",
        scatter_dimension=0,
        tiled=True,
    )
    query_b = to_blocks(queries, KEY_CHANNELS)
    key_b = to_blocks(key_rows, KEY_CHANNELS)
    value_b = to_blocks(values, DV)
    grad_b = to_blocks(out_grad, DV)
    cumulative = jnp.cumsum(to_blocks(log_decay, KEY_CHANNELS), axis=2)
    block_totals = cumulative[:, :, -1, :]
    prefix = jnp.cumsum(block_totals, axis=0) - block_totals
    span_cumul = cumulative + prefix[:, :, None, :]
    span_factor = jnp.exp(jnp.sum(block_totals, axis=0))
    span_term = jnp.einsum(
        "nhcd,nhcv->hdv", query_b * jnp.exp(span_cumul), grad_b, precision=highest
    )

    def forward(carried, inputs):
        key_blk, value_blk, cumul_blk = inputs
        final_log = cumul_blk[:, -1, :]
        state_after = jnp.exp(final_log)[:, :, None] * carried + jnp.einsum(
            "hsd,hsv->hdv",
            key_blk * jnp.exp(final_log[:, None, :] - cumul_blk),
            value_blk,
            precision=highest,
        )
        return (state_after, carried)

    span_end, starts = lax.scan(forward, saved_state[0], (key_b, value_b, cumulative))

    def combine_maps(farther, nearer):
        return (nearer[0] * farther[0], nearer[0][:, :, None] * farther[1] + nearer[1])

    identity = (jnp.ones_like(span_factor), jnp.zeros_like(span_term))
    scanned = entering((span_factor, span_term), "sp", combine_maps, identity)
    from_later = scanned[1]

    def backward(carried, inputs):
        return block_grads(*inputs, carried)

    _, (query_grads, key_grads, value_grads, cumul_grads) = lax.scan(
        backward, from_later, (query_b, key_b, value_b, cumulative, grad_b, starts), reverse=True
    )
    cross_term = jnp.sum(span_end * from_later, axis=2).reshape(1, -1)
    flat_cum = from_blocks(cumul_grads)
    token_positions = jnp.arange(flat_cum.shape[0], dtype=jnp.int32)
    later_mask = (token_positions[None, :] >= token_positions[:, None]).astype(jnp.float32)
    grad_decay = jnp.dot(later_mask, flat_cum, precision=highest) + cross_term
    return (
        grad_gate,
        grad_up,
        grad_down,
        grad_outproj,
        from_blocks(query_grads).astype(jnp.bfloat16),
        from_blocks(key_grads).astype(jnp.bfloat16),
        from_blocks(value_grads).astype(jnp.bfloat16),
        grad_decay,
    )


def solution(mesh):
    placed = (
        P("sp", None),
        P("sp", None),
        P("sp", None),
        P("sp", None),
        P("sp", None, "tp"),
        P("sp", None, "tp"),
        P("sp", "tp", None),
        P("tp", None),
        P("sp", "tp"),
        P("sp", "tp"),
        P("sp", "tp"),
        P("sp", "tp"),
        P("sp", "tp"),
        P("sp", "tp", None, None),
    )
    return jax.shard_map(
        body,
        mesh=mesh,
        in_specs=placed,
        out_specs=(
            P("sp", None, "tp"),
            P("sp", None, "tp"),
            P("sp", "tp", None),
            P("sp", "tp"),
            P("sp", "tp"),
            P("sp", "tp"),
            P("sp", "tp"),
            P("sp", "tp"),
        ),
        check_vma=False,
    )
```

profile of v0, /device:TPU:0, one launch (start us, length us, event | category | flops | bytes accessed | tf_op | source)
XLA Modules:
  0.0 823.2 jit_solution(12827998043781431697)
XLA Ops:
  38.2 28.3 %all-to-all-done = bf16[16,48,1024]{2,1,0:T(8,128)(2,1)} async-done(((bf16[16,48,1024]{2,1,0:T(8,128)(2,1)}), bf16[16,48,1024]{2,1,0:T(8,128)(2,1)}, u32[]{:S(2)}, u32[]{:S(2)}) %all-to-all-start) | async-done | bytes 1572896 | tf_op jit(solution)/shard_map/all_to_all | solution.py:145
  68.4 44.9 %all_to_all.33 = bf16[16,48,1024]{2,1,0:T(8,128)(2,1)} all-to-all(bf16[16,48,1024]{2,1,0:T(8,128)(2,1)S(1)} %bitcast.292), channel_id=1, replica_groups=mesh['sp'=16,'tp'=2] {'sp'}, dimensions={0} | all-to-all | bytes 3145728 | tf_op jit(solution)/shard_map/all_to_all | solution.py:146
  124.1 38.5 %all-gather.9.cloned.1.call-done = bf16[1,768,2048]{2,1,0:T(8,128)(2,1)} async-done(((bf16[1,768,1024]{2,1,0:T(8,128)(2,1)}), bf16[1,768,2048]{2,1,0:T(8,128)(2,1)}) %all-gather.9.cloned.1.call-update) | async-done | bytes 3145744 | tf_op jit(solution)/shard_map/all_gather | solution.py:150
  173.9 43.6 %reduce-scatter.3.cloned.1.call-done = bf16[1,768,1024]{2,1,0:T(8,128)(2,1)} async-done(((bf16[1,768,2048]{2,1,0:T(8,128)(2,1)}), bf16[1,768,1024]{2,1,0:T(8,128)(2,1)}) %reduce-scatter.3.cloned.1.call-update) | async-done | bytes 1572880 | tf_op jit(solution)/shard_map/reduce_scatter | solution.py:173
  223.5 11.6 %reduce.11 = bf16[768,1024]{1,0:T(8,128)(2,1)S(1)} reduce(bf16[768,1,1024]{2,1,0:T(2,128)(2,1)} %bitcast.287, bf16[]{:T(256)} %broadcast.135), dimensions={1}, to_apply=%bitcast.216.reduce_sub_computation | reduce | bytes 3145730
  243.4 31.4 %all-to-all-done.2 = bf16[16,2,24576]{2,1,0:T(2,128)(2,1)S(1)} async-done(((bf16[16,2,24576]{2,1,0:T(2,128)(2,1)}), bf16[16,2,24576]{2,1,0:T(2,128)(2,1)S(1)}, u32[]{:S(2)}, u32[]{:S(2)}) %all-to-all-start.2) | async-done | bytes 1572896 | tf_op jit(solution)/shard_map/all_to_all | solution.py:176
  300.5 26.1 %fusion.96 = f32[4,16,64,32]{3,1,2,0:T(8,128)S(1)} fusion(f32[4,16,64,32]{3,1,2,0:T(8,128)S(1)} %copy-done.9), kind=kOutput, calls=%fused_computation.156 | output fusion | flops 8257536 | bytes 1048576 | tf_op jit(solution)/shard_map/jit(cumsum)/reduce_window_sum | solution.py:195
  338.8 19.4 %while.49 = (s32[]{:T(128)}, f32[16,32,64]{2,1,0:T(8,128)S(1)}, f32[4,16,32,64]{3,2,1,0:T(8,128)}, f32[4,16,64,32]{3,1,2,0:T(8,128)S(1)}, f32[4,16,64,32]{2,0,3,...) while((s32[]{:T(128)}, f32[16,32,64]{2,1,0:T(8,128)S(1)}, f32[4,16,32,64]{3,2,1,0:T(8,128)}, ...), condition=%wide.region_13.15_spmd, body=%wide.region_12.14_spmd.sunk | while | flops 25296896 | bytes 2502761 | solution.py:215
  364.2 26.2 %all-gather = f32[256,32]{1,0:T(8,128)S(1)} all-gather(f32[16,32]{1,0:T(8,128)S(1)} %exp.72), channel_id=2, replica_groups=mesh['sp'=16,'tp'=2] {'sp'}, dimensions={0}, use_global_device_ids=true | all-gather | bytes 34816 | tf_op jit(solution)/shard_map/all_gather | solution.py:18
  408.6 18.0 %while.48 = (s32[]{:T(128)}, f32[16,32,64]{2,1,0:T(8,128)S(1)}, s32[]{:T(128)}, f32[16,16,32]{2,1,0:T(8,128)S(1)}, f32[16,16,32,64]{3,2,1,0:T(8,128)}, /*index=5*/s32[]{:T(128)}, s32[]{:T(128)}, s32[]{:T(128)}, s32[]{:T(128)}) while((s32[]{:T(128)}, f32[16,32,64]{2,1,0:T(8,128)S(1)}, s32[]{:T(128)}, f32[16,16,32]{2,1,0:T(8,128)S(1)}, ...), condition=%wide.region_11.13_spmd, body=%wide.region_10.12_spmd.sunk | while | flops 65542 | bytes 399515 | solution.py:27
  429.0 373.9 %while.50 = (s32[]{:T(128)}, f32[16,32,64]{2,1,0:T(8,128)S(1)}, bf16[4,16,64,32]{2,3,1,0:T(8,128)(2,1)}, bf16[4,16,64,32]{2,3,1,0:T(8,128)(2,1)}, bf16[4,16,64,6...) while((s32[]{:T(128)}, f32[16,32,64]{2,1,0:T(8,128)S(1)}, ...), condition=%wide.region_15.17_spmd, body=%wide.region_14.16_spmd.sunk | while | flops 233148416 | bytes 89160528 | solution.py:227
  435.6 10.0 %multiply_reduce_fusion.5 = f32[16,64,32]{1,2,0:T(8,128)S(1)} fusion(f32[16,64,64]{2,1,0:T(8,128)S(1)} %fusion.146, f32[16,64,32]{2,1,0:T(8,128)S(1)} %copy.243, f32[16,64,32]{1,2,0:T(8,128)S(1)} %get-tuple-element.734, f32[16,64,32]{2,1,0:T(8,128)S(1)} %copy.244, pred[64,64]{1,0:T(8,128)(4,1)S(1)} %iota_compare_fusion.6), kind=kLoop, calls=%fused_computation.20.clone.1 | loop fusion | flops 12550144 | bytes 790528 | tf_op jit(solution)/shard_map/while/body/eval_jaxpr/hts,htd,htsd->hsd/dot_general | solution.py:59
  449.4 12.5 %exponential_select_fusion.2 = (f32[16,64,64,32]{2,3,1,0:T(8,128)}, f32[16,64,32,64]{3,2,1,0:T(8,128)}) fusion(f32[16,64,32]{1,2,0:T(8,128)S(1)} %get-tuple-element.734, f32[16,64,32]{2,1,0:T(8,128)S(1)} %copy.244, pred[64,64]{1,0:T(8,128)(4,1)S(1)} %iota_compare_fusion.6), kind=kLoop, calls=%fused_computation.22.clone.3 | loop fusion | flops 6291456 | bytes 17043456 | tf_op jit(solution)/shard_map/while/body/eval_jaxpr/jit(_where)/select_n | solution.py:50
  461.9 19.8 %copy.245 = f32[16,64,32,64]{1,2,3,0:T(8,128)} copy(f32[16,64,32,64]{3,2,1,0:T(8,128)} %get-tuple-element.736) | data formatting | bytes 16777216 | tf_op jit(solution)/shard_map/while
  482.2 8.0 multiply_reduce_fusion.6
  493.8 18.6 %copy.248 = f32[16,64,64,32]{1,2,3,0:T(8,128)} copy(f32[16,64,64,32]{2,3,1,0:T(8,128)} %get-tuple-element.739) | data formatting | bytes 16777216 | tf_op jit(solution)/shard_map/while
  512.5 7.7 fusion.149
  529.4 10.0 %multiply_reduce_fusion.5 = f32[16,64,32]{1,2,0:T(8,128)S(1)} fusion(f32[16,64,64]{2,1,0:T(8,128)S(1)} %fusion.146, f32[16,64,32]{2,1,0:T(8,128)S(1)} %copy.243, f32[16,64,32]{1,2,0:T(8,128)S(1)} %get-tuple-element.734, f32[16,64,32]{2,1,0:T(8,128)S(1)} %copy.244, pred[64,64]{1,0:T(8,128)(4,1)S(1)} %iota_compare_fusion.6), kind=kLoop, calls=%fused_computation.20.clone.1 | loop fusion | flops 12550144 | bytes 790528 | tf_op jit(solution)/shard_map/while/body/eval_jaxpr/hts,htd,htsd->hsd/dot_general | solution.py:59
  543.2 12.5 %exponential_select_fusion.2 = (f32[16,64,64,32]{2,3,1,0:T(8,128)}, f32[16,64,32,64]{3,2,1,0:T(8,128)}) fusion(f32[16,64,32]{1,2,0:T(8,128)S(1)} %get-tuple-element.734, f32[16,64,32]{2,1,0:T(8,128)S(1)} %copy.244, pred[64,64]{1,0:T(8,128)(4,1)S(1)} %iota_compare_fusion.6), kind=kLoop, calls=%fused_computation.22.clone.3 | loop fusion | flops 6291456 | bytes 17043456 | tf_op jit(solution)/shard_map/while/body/eval_jaxpr/jit(_where)/select_n | solution.py:50
  555.7 19.6 %copy.245 = f32[16,64,32,64]{1,2,3,0:T(8,128)} copy(f32[16,64,32,64]{3,2,1,0:T(8,128)} %get-tuple-element.736) | data formatting | bytes 16777216 | tf_op jit(solution)/shard_map/while
  587.1 18.6 %copy.248 = f32[16,64,64,32]{1,2,3,0:T(8,128)} copy(f32[16,64,64,32]{2,3,1,0:T(8,128)} %get-tuple-element.739) | data formatting | bytes 16777216 | tf_op jit(solution)/shard_map/while
  605.7 7.7 fusion.149
  622.7 10.0 %multiply_reduce_fusion.5 = f32[16,64,32]{1,2,0:T(8,128)S(1)} fusion(f32[16,64,64]{2,1,0:T(8,128)S(1)} %fusion.146, f32[16,64,32]{2,1,0:T(8,128)S(1)} %copy.243, f32[16,64,32]{1,2,0:T(8,128)S(1)} %get-tuple-element.734, f32[16,64,32]{2,1,0:T(8,128)S(1)} %copy.244, pred[64,64]{1,0:T(8,128)(4,1)S(1)} %iota_compare_fusion.6), kind=kLoop, calls=%fused_computation.20.clone.1 | loop fusion | flops 12550144 | bytes 790528 | tf_op jit(solution)/shard_map/while/body/eval_jaxpr/hts,htd,htsd->hsd/dot_general | solution.py:59
  636.5 12.5 %exponential_select_fusion.2 = (f32[16,64,64,32]{2,3,1,0:T(8,128)}, f32[16,64,32,64]{3,2,1,0:T(8,128)}) fusion(f32[16,64,32]{1,2,0:T(8,128)S(1)} %get-tuple-element.734, f32[16,64,32]{2,1,0:T(8,128)S(1)} %copy.244, pred[64,64]{1,0:T(8,128)(4,1)S(1)} %iota_compare_fusion.6), kind=kLoop, calls=%fused_computation.22.clone.3 | loop fusion | flops 6291456 | bytes 17043456 | tf_op jit(solution)/shard_map/while/body/eval_jaxpr/jit(_where)/select_n | solution.py:50
  649.0 19.6 %copy.245 = f32[16,64,32,64]{1,2,3,0:T(8,128)} copy(f32[16,64,32,64]{3,2,1,0:T(8,128)} %get-tuple-element.736) | data formatting | bytes 16777216 | tf_op jit(solution)/shard_map/while
  680.4 18.6 %copy.248 = f32[16,64,64,32]{1,2,3,0:T(8,128)} copy(f32[16,64,64,32]{2,3,1,0:T(8,128)} %get-tuple-element.739) | data formatting | bytes 16777216 | tf_op jit(solution)/shard_map/while
  699.0 7.7 fusion.149
  716.0 10.0 %multiply_reduce_fusion.5 = f32[16,64,32]{1,2,0:T(8,128)S(1)} fusion(f32[16,64,64]{2,1,0:T(8,128)S(1)} %fusion.146, f32[16,64,32]{2,1,0:T(8,128)S(1)} %copy.243, f32[16,64,32]{1,2,0:T(8,128)S(1)} %get-tuple-element.734, f32[16,64,32]{2,1,0:T(8,128)S(1)} %copy.244, pred[64,64]{1,0:T(8,128)(4,1)S(1)} %iota_compare_fusion.6), kind=kLoop, calls=%fused_computation.20.clone.1 | loop fusion | flops 12550144 | bytes 790528 | tf_op jit(solution)/shard_map/while/body/eval_jaxpr/hts,htd,htsd->hsd/dot_general | solution.py:59
  729.7 12.5 %exponential_select_fusion.2 = (f32[16,64,64,32]{2,3,1,0:T(8,128)}, f32[16,64,32,64]{3,2,1,0:T(8,128)}) fusion(f32[16,64,32]{1,2,0:T(8,128)S(1)} %get-tuple-element.734, f32[16,64,32]{2,1,0:T(8,128)S(1)} %copy.244, pred[64,64]{1,0:T(8,128)(4,1)S(1)} %iota_compare_fusion.6), kind=kLoop, calls=%fused_computation.22.clone.3 | loop fusion | flops 6291456 | bytes 17043456 | tf_op jit(solution)/shard_map/while/body/eval_jaxpr/jit(_where)/select_n | solution.py:50
  742.3 19.6 %copy.245 = f32[16,64,32,64]{1,2,3,0:T(8,128)} copy(f32[16,64,32,64]{3,2,1,0:T(8,128)} %get-tuple-element.736) | data formatting | bytes 16777216 | tf_op jit(solution)/shard_map/while
  773.7 18.6 %copy.248 = f32[16,64,64,32]{1,2,3,0:T(8,128)} copy(f32[16,64,64,32]{2,3,1,0:T(8,128)} %get-tuple-element.739) | data formatting | bytes 16777216 | tf_op jit(solution)/shard_map/while
  792.3 7.7 fusion.149
  (342 shorter events, 273.6 us)
Async XLA Ops:
  7.2 108.9 %copy-start = (bf16[1,2048,512]{2,1,0:T(8,128)(2,1)S(1)}, bf16[1,2048,512]{2,1,0:T(8,128)(2,1)}, u32[]{:S(2)}) copy-start(bf16[1,2048,512]{2,1,0:T(8,128)(2,1)} %param.26) | copy-start | bytes 6291460
  27.2 39.3 %all-to-all-start = ((bf16[16,48,1024]{2,1,0:T(8,128)(2,1)}), bf16[16,48,1024]{2,1,0:T(8,128)(2,1)}, u32[]{:S(2)}, u32[]{:S(2)}) async-start(bf16[16,48,1024]{2,1,0:T(8,128)(2,1)} %bitcast.293), calls=%async_computation | async-start | bytes 3145728 | tf_op jit(solution)/shard_map/all_to_all | solution.py:145
  34.6 81.5 %all-gather.7.cloned.1.call-start = ((), (), s32[]{:S(2)}) async-start(), calls=%async_computation.5 | async-start | bytes 4718592 | tf_op jit(solution)/shard_map/all_gather | solution.py:149
  66.5 96.0 %all-gather.9.cloned.1.call-start = ((), (), s32[]{:S(2)}) async-start(), calls=%async_computation.6 | async-start | bytes 4718592 | tf_op jit(solution)/shard_map/all_gather | solution.py:150
  113.4 104.1 %reduce-scatter.3.cloned.1.call-start = ((), (), s32[]{:S(2)}) async-start(), calls=%async_computation.7 | async-start | bytes 4718592 | tf_op jit(solution)/shard_map/reduce_scatter | solution.py:173
  237.2 6.0 copy-start.31
  237.2 37.6 %all-to-all-start.2 = ((bf16[16,2,24576]{2,1,0:T(2,128)(2,1)}), bf16[16,2,24576]{2,1,0:T(2,128)(2,1)S(1)}, u32[]{:S(2)}, u32[]{:S(2)}) async-start(bf16[16,2,24576]{2,1,0:T(2,128)(2,1)} %reshape.325), calls=%async_computation.3 | async-start | bytes 3145728 | tf_op jit(solution)/shard_map/all_to_all | solution.py:176
  242.9 85.3 %all-gather.11.cloned.1.call-start = ((), (), s32[]{:S(2)}) async-start(), calls=%async_computation.8 | async-start | bytes 1572864 | tf_op jit(solution)/shard_map/all_gather | solution.py:179
  291.8 116.8 %all-gather.13.cloned.1.call-start = ((), (), s32[]{:S(2)}) async-start(), calls=%async_computation.10 | async-start | bytes 4456448 | tf_op jit(solution)/shard_map/all_gather | solution.py:18
  300.5 26.1 %copy-start.5 = (f32[4,64,16,32]{3,2,1,0:T(8,128)S(1)}, f32[4,64,16,32]{3,2,1,0:T(8,128)}, u32[]{:S(2)}) copy-start(f32[4,64,16,32]{3,2,1,0:T(8,128)} %reshape.320) | copy-start | bytes 1572868
  333.6 5.2 copy-start.4
  338.7 477.1 %reduce-scatter.5.cloned.1.call-start = ((), (), s32[]{:S(2)}) async-start(), calls=%async_computation.9 | async-start | bytes 8912896 | tf_op jit(solution)/shard_map/reduce_scatter | solution.py:183
  360.1 30.3 %copy-start.25 = (bf16[768,512]{1,0:T(8,128)(2,1)S(1)}, bf16[768,512]{1,0:T(8,128)(2,1)}, u32[]{:S(2)}) copy-start(bf16[768,512]{1,0:T(8,128)(2,1)} %copy-done.24) | copy-start | bytes 2359300
  390.4 5.3 copy-start.23
  390.5 5.3 copy-start.33
  482.1 8.0 copy-start.11
  482.1 8.0 copy-start.16
  493.8 18.6 %copy-start.12 = (bf16[4,16,64,32]{2,3,1,0:T(8,128)(2,1)}, bf16[4,16,64,32]{2,3,1,0:T(8,128)(2,1)S(1)}, u32[]{:S(2)}) copy-start(bf16[4,16,64,32]{2,3,1,0:T(8,128)(2,1)S(1)} %get-tuple-element.820) | copy-start | bytes 786436 | tf_op jit(solution)/shard_map/while
  512.5 7.7 copy-start.13
  575.7 7.7 copy-start.11
  575.8 7.7 copy-start.16
  587.1 18.6 %copy-start.12 = (bf16[4,16,64,32]{2,3,1,0:T(8,128)(2,1)}, bf16[4,16,64,32]{2,3,1,0:T(8,128)(2,1)S(1)}, u32[]{:S(2)}) copy-start(bf16[4,16,64,32]{2,3,1,0:T(8,128)(2,1)S(1)} %get-tuple-element.820) | copy-start | bytes 786436 | tf_op jit(solution)/shard_map/while
  605.7 7.7 copy-start.13
  669.0 7.7 copy-start.11
  669.0 7.7 copy-start.16
  680.4 18.6 %copy-start.12 = (bf16[4,16,64,32]{2,3,1,0:T(8,128)(2,1)}, bf16[4,16,64,32]{2,3,1,0:T(8,128)(2,1)S(1)}, u32[]{:S(2)}) copy-start(bf16[4,16,64,32]{2,3,1,0:T(8,128)(2,1)S(1)} %get-tuple-element.820) | copy-start | bytes 786436 | tf_op jit(solution)/shard_map/while
  699.0 7.7 copy-start.13
  762.3 7.7 copy-start.11
  762.3 7.7 copy-start.16
  773.7 18.6 %copy-start.12 = (bf16[4,16,64,32]{2,3,1,0:T(8,128)(2,1)}, bf16[4,16,64,32]{2,3,1,0:T(8,128)(2,1)S(1)}, u32[]{:S(2)}) copy-start(bf16[4,16,64,32]{2,3,1,0:T(8,128)(2,1)S(1)} %get-tuple-element.820) | copy-start | bytes 786436 | tf_op jit(solution)/shard_map/while
  792.3 7.7 copy-start.13
  809.5 6.4 copy-start.1
  (31 other events, 79.3 us)
Sparse Core Ops, SparseCore 0:
  66.6 49.3 all-gather.6
  117.6 44.8 all-gather.8
  174.0 43.4 reduce-scatter.2
  291.9 24.8 all-gather.10
  338.8 54.4 all-gather.12
  408.7 99.6 reduce-scatter.4
where the time goes:
time: 832 us; the launch traced here: 823 us
  local copies, waits for them, and re-layouts  255 us (31%)
  other arithmetic  221 us (27%)
  waiting for transfers between devices  144 us (17%)
  matrix products  100 us (12%)
  blocking collectives  71.1 us (9%)
  between operations  15.2 us (2%)
  starting transfers between devices  13.8 us (2%)
    while x56, local copies, waits for them, and re-layouts  160 us
    select_n x4, other arithmetic, block_grads(): jnp.where(causal_mask, jnp.exp(jnp.where(causal_mask, log_gaps, 0.0)), 0.0)  50.1 us
    all_to_all x1, blocking collectives, body(): lax.all_to_all(rows_cot, 'sp', split_axis=0, concat_axis=1, tiled=True)  44.9 us
    reduce_scatter x1, waiting for transfers between devices, body(): lax.psum_scatter(partial_value.astype(jnp.bfloat16), 'tp', scatter_dimens...  43.6 us
    dot_general x4, other arithmetic, block_grads(): jnp.einsum('hts,htd,htsd->hsd', couplings, queries, decays, precision=hig...  40 us
    all_gather x1, waiting for transfers between devices, body(): lax.all_gather(got_cot, 'tp', axis=2, tiled=True)  38.5 us
    all_to_all x1, waiting for transfers between devices, body(): lax.all_to_all(summed, 'sp', split_axis=1, concat_axis=0, tiled=True)  31.4 us
    dot_general x4, other arithmetic, block_grads(): jnp.einsum('hts,hsd,htsd->htd', couplings, key_rows, decays, precision=hi...  30.9 us
  transfers between devices with their start and end apart: 8, of which 5 were waited for; matrix products, arithmetic and copies ran while one was open for 60% of the time, Pallas kernels for 0%

commit v1 on v0

v1 whole, which is shorter than its diff:
```python
import functools

import jax
import jax.numpy as jnp
from jax import lax
from jax.experimental import pallas as pl
from jax.experimental.pallas import tpu as pltpu
from jax.sharding import PartitionSpec as P

KEY_CHANNELS = 32
DV = 64
BLOCK = 64
LANES = 128
GROUP = LANES // KEY_CHANNELS
GV = GROUP * DV

f32 = jnp.float32
bf16 = jnp.bfloat16


def dot(a, b, ca, cb):
    return lax.dot_general(a, b, (((ca,), (cb,)), ((), ())), preferred_element_type=f32)


def iota(shape, dim):
    return lax.broadcasted_iota(jnp.int32, shape, dim)


def state_mask():
    return (iota((GV, LANES), 0) // DV) == (iota((GV, LANES), 1) // KEY_CHANNELS)


def tile(a):
    return jnp.concatenate([a] * GROUP, axis=0)


def fold(a):
    rows = a.shape[0] // GROUP
    total = a[:rows]
    for h in range(1, GROUP):
        total = total + a[h * rows : (h + 1) * rows]
    return total


def split_dot(mask, a, parts):
    total = None
    for _ in range(parts):
        piece = a.astype(bf16)
        term = dot(mask, piece, 1, 0)
        total = term if total is None else total + term
        a = a - piece.astype(f32)
    return total


def tri(lower):
    r, c = iota((BLOCK, BLOCK), 0), iota((BLOCK, BLOCK), 1)
    return jnp.where((r >= c) if lower else (c >= r), 1.0, 0.0).astype(bf16)


def pre_kernel(k_ref, v_ref, ld_ref, s_ref, cum_ref, st_ref):
    blocks = k_ref.shape[0] // BLOCK
    mask = state_mask()
    lower = tri(True)
    state = s_ref[...]
    for n in range(blocks):
        rows = pl.ds(n * BLOCK, BLOCK)
        cum = split_dot(lower, ld_ref[rows, :], 3)
        cum_ref[rows, :] = cum
        st_ref[n] = state
        fin = cum[BLOCK - 1 : BLOCK]
        kd = (k_ref[rows, :].astype(f32) * jnp.exp(fin - cum)).astype(bf16)
        state = jnp.exp(fin) * state + fold(jnp.where(mask, dot(v_ref[rows, :], kd, 0, 0), 0.0))
    st_ref[blocks] = state


def span_kernel(q_ref, g_ref, cum_ref, t_ref):
    blocks = q_ref.shape[0] // BLOCK
    mask = state_mask()
    total = jnp.zeros((DV, LANES), f32)
    log = jnp.zeros((1, LANES), f32)
    for n in reversed(range(blocks)):
        rows = pl.ds(n * BLOCK, BLOCK)
        cum = cum_ref[rows, :]
        fin = cum[BLOCK - 1 : BLOCK]
        log = log + fin
        qd = (q_ref[rows, :].astype(f32) * jnp.exp(cum)).astype(bf16)
        total = jnp.exp(fin) * total + fold(jnp.where(mask, dot(g_ref[rows, :], qd, 0, 0), 0.0))
    t_ref[0:DV, :] = total
    t_ref[DV : DV + 8, :] = jnp.broadcast_to(jnp.exp(log), (8, LANES))


def main_kernel(
    me_ref, q_ref, k_ref, v_ref, g_ref, cum_ref, st_ref, far_ref, dq_ref, dk_ref, dv_ref, dd_ref
):
    blocks = q_ref.shape[0] // BLOCK
    spans = far_ref.shape[0]
    mask = state_mask()
    vmask = (iota((GROUP * BLOCK, GV), 0) // BLOCK) == (iota((GROUP * BLOCK, GV), 1) // DV)
    qmask = (iota((GROUP * BLOCK, LANES), 0) // BLOCK) == (
        iota((GROUP * BLOCK, LANES), 1) // KEY_CHANNELS
    )
    causal = (iota((GROUP * BLOCK, BLOCK), 0) % BLOCK) >= iota((GROUP * BLOCK, BLOCK), 1)
    upper = tri(False)
    me = me_ref[0]

    def one(i, later):
        source = spans - 1 - i
        far = far_ref[source]
        nearer = far[DV : DV + 1] * later + far[0:DV]
        return jnp.where(source > me, nearer, later)

    later = lax.fori_loop(0, spans, one, jnp.zeros((DV, LANES), f32))
    carry = jnp.sum(st_ref[blocks] * later, axis=0, keepdims=True)
    for n in reversed(range(blocks)):
        rows = pl.ds(n * BLOCK, BLOCK)
        q = q_ref[rows, :].astype(f32)
        k = k_ref[rows, :].astype(f32)
        v = v_ref[rows, :]
        g = g_ref[rows, :]
        cum = cum_ref[rows, :]
        mid = 0.5 * cum[BLOCK - 1 : BLOCK]
        half = jnp.exp(mid)
        eq = jnp.exp(cum - mid)
        ek = jnp.exp(mid - cum)
        kt = (k * ek).astype(bf16)
        qs = jnp.where(qmask, tile(q * eq), 0.0).astype(bf16)
        gs = jnp.where(vmask, tile(g.astype(f32)), 0.0).astype(bf16)
        scores = jnp.where(causal, dot(qs, kt, 1, 1), 0.0).astype(bf16)
        couple = jnp.where(causal, dot(gs, v, 1, 1), 0.0).astype(bf16)
        dq_in = fold(jnp.where(qmask, dot(couple, kt, 1, 0), 0.0))
        dk_in = dot(couple, qs, 0, 0)
        dv_in = dot(scores, gs, 0, 0)
        state = jnp.where(mask, tile(st_ref[n]), 0.0).astype(bf16)
        after = jnp.where(mask, tile(later), 0.0).astype(bf16)
        dq = eq * (dq_in + half * dot(g, state, 1, 0))
        dk = ek * (dk_in + half * dot(v, after, 1, 0))
        dv = dv_in + dot((k * (ek * half)).astype(bf16), after, 1, 1)
        dq_ref[rows, :] = dq.astype(bf16)
        dk_ref[rows, :] = dk.astype(bf16)
        dv_ref[rows, :] = dv.astype(bf16)
        suffix = split_dot(upper, q * dq - k * dk, 3) + carry
        dd_ref[rows, :] = suffix
        carry = suffix[0:1]
        qd = (q * (eq * half)).astype(bf16)
        later = half * half * later + fold(jnp.where(mask, dot(g, qd, 0, 0), 0.0))


def params(**more):
    return pltpu.CompilerParams(dimension_semantics=("arbitrary",), **more)


def cols(rows, width):
    return pl.BlockSpec((rows, width), lambda i, *_: (0, i))


def cols3(lead, rows):
    return pl.BlockSpec((lead, rows, LANES), lambda i, *_: (0, 0, i))


def mixer_pre(key_rows, values, log_decay, saved):
    tok, hk = key_rows.shape
    blocks = tok // BLOCK
    return pl.pallas_call(
        pre_kernel,
        grid=(hk // LANES,),
        in_specs=[cols(tok, LANES), cols(tok, GV), cols(tok, LANES), cols(DV, LANES)],
        out_specs=[cols(tok, LANES), cols3(blocks + 1, DV)],
        out_shape=[
            jax.ShapeDtypeStruct((tok, hk), f32),
            jax.ShapeDtypeStruct((blocks + 1, DV, hk), f32),
        ],
        compiler_params=params(),
        cost_estimate=pl.CostEstimate(flops=10**9, bytes_accessed=4 * 10**6, transcendentals=0),
        name="mixer_pre",
    )(key_rows, values, log_decay, saved)


def mixer_span(queries, out_grad, cum):
    tok, hk = queries.shape
    return pl.pallas_call(
        span_kernel,
        grid=(hk // LANES,),
        in_specs=[cols(tok, LANES), cols(tok, GV), cols(tok, LANES)],
        out_specs=cols(DV + 8, LANES),
        out_shape=jax.ShapeDtypeStruct((DV + 8, hk), f32),
        compiler_params=params(),
        cost_estimate=pl.CostEstimate(flops=10**8, bytes_accessed=2 * 10**6, transcendentals=0),
        name="mixer_span",
    )(queries, out_grad, cum)


def mixer_main(me, queries, key_rows, values, out_grad, cum, states, far):
    tok, hk = queries.shape
    hv = values.shape[1]
    blocks = tok // BLOCK
    return pl.pallas_call(
        main_kernel,
        grid_spec=pltpu.PrefetchScalarGridSpec(
            num_scalar_prefetch=1,
            grid=(hk // LANES,),
            in_specs=[
                cols(tok, LANES),
                cols(tok, LANES),
                cols(tok, GV),
                cols(tok, GV),
                cols(tok, LANES),
                cols3(blocks + 1, DV),
                cols3(far.shape[0], DV + 8),
            ],
            out_specs=[cols(tok, LANES), cols(tok, LANES), cols(tok, GV), cols(tok, LANES)],
        ),
        out_shape=[
            jax.ShapeDtypeStruct((tok, hk), bf16),
            jax.ShapeDtypeStruct((tok, hk), bf16),
            jax.ShapeDtypeStruct((tok, hv), bf16),
            jax.ShapeDtypeStruct((tok, hk), f32),
        ],
        compiler_params=params(),
        cost_estimate=pl.CostEstimate(
            flops=4 * 10**9, bytes_accessed=6 * 10**6, transcendentals=0
        ),
        name="mixer_main",
    )(me, queries, key_rows, values, out_grad, cum, states, far)


def dispatch_places(routes, experts, capacity):
    tok, top = routes.shape
    flat = routes.reshape(-1)
    count = flat.shape[0]
    onehot = flat[:, None] == jnp.arange(experts, dtype=jnp.int32)[None, :]
    earlier = jnp.arange(count)[:, None] > jnp.arange(count)[None, :]
    before = jnp.dot(
        earlier.astype(bf16), onehot.astype(bf16), preferred_element_type=f32
    )
    ranks = jnp.sum(jnp.where(onehot, before, 0.0), axis=1).astype(jnp.int32)
    return (flat * capacity + ranks).reshape(tok, top)


def body(
    layer_cot,
    moe_input,
    routes,
    route_weights,
    gate_proj,
    up_proj,
    down_proj,
    out_proj,
    mixer_out,
    queries,
    key_rows,
    values,
    log_decay,
    saved_state,
):
    sp_count = lax.axis_size("sp")
    tp_count = lax.axis_size("tp")
    local_experts = gate_proj.shape[0]
    experts = local_experts * sp_count
    tok_local, model_width = layer_cot.shape
    top_count = routes.shape[1]
    capacity = 3 * tok_local // experts
    slots = experts * capacity
    quarter = model_width // tp_count
    tp_rank = lax.axis_index("tp")

    places = dispatch_places(routes, experts, capacity)
    slot_ids = jnp.arange(slots, dtype=jnp.int32)
    hits = [slot_ids[:, None] == places[None, :, j] for j in range(top_count)]
    picks = functools.reduce(jnp.logical_or, hits).astype(bf16)
    slot_weights = sum(
        jnp.sum(jnp.where(hits[j], route_weights[None, :, j], 0.0), axis=1)
        for j in range(top_count)
    )
    part_in = lax.dynamic_slice_in_dim(moe_input, tp_rank * quarter, quarter, 1)
    part_cot = lax.dynamic_slice_in_dim(layer_cot, tp_rank * quarter, quarter, 1)
    rows_in = jnp.dot(picks, part_in, preferred_element_type=f32).astype(bf16)
    rows_cot = (
        slot_weights[:, None] * jnp.dot(picks, part_cot, preferred_element_type=f32)
    ).astype(bf16)
    rows_in = rows_in.reshape(experts, capacity, quarter)
    rows_cot = rows_cot.reshape(experts, capacity, quarter)
    got_in, got_cot = (
        lax.all_to_all(rows_in, "sp", split_axis=0, concat_axis=1, tiled=True),
        lax.all_to_all(rows_cot, "sp", split_axis=0, concat_axis=1, tiled=True),
    )
    got_in, got_cot = (
        lax.all_gather(got_in, "tp", axis=2, tiled=True),
        lax.all_gather(got_cot, "tp", axis=2, tiled=True),
    )
    saved = saved_state[0].transpose(2, 0, 1).reshape(DV, -1)
    cum, states = mixer_pre(key_rows, values, log_decay, saved)
    all_mixer = lax.all_gather(mixer_out, "sp", axis=0, tiled=True)

    pre_gate = jnp.einsum("erd,edf->erf", got_in, gate_proj, preferred_element_type=f32)
    pre_up = jnp.einsum("erd,edf->erf", got_in, up_proj, preferred_element_type=f32)
    sigmoid_gate = jax.nn.sigmoid(pre_gate)
    hidden = (pre_gate * sigmoid_gate * pre_up).astype(bf16)
    grad_hidden = jnp.einsum("erd,efd->erf", got_cot, down_proj, preferred_element_type=f32)
    grad_down = jnp.einsum("erf,erd->efd", hidden, got_cot, preferred_element_type=f32).astype(
        bf16
    )
    grad_pre_gate = (
        grad_hidden * pre_up * sigmoid_gate * (1.0 + pre_gate * (1.0 - sigmoid_gate))
    ).astype(bf16)
    grad_pre_up = (grad_hidden * pre_gate * sigmoid_gate).astype(bf16)
    grad_gate = jnp.einsum("erd,erf->edf", got_in, grad_pre_gate, preferred_element_type=f32).astype(
        bf16
    )
    grad_up = jnp.einsum("erd,erf->edf", got_in, grad_pre_up, preferred_element_type=f32).astype(
        bf16
    )
    partial_value = jnp.einsum(
        "erf,edf->erd", grad_pre_gate, gate_proj, preferred_element_type=f32
    ) + jnp.einsum("erf,edf->erd", grad_pre_up, up_proj, preferred_element_type=f32)
    summed = lax.psum_scatter(partial_value.astype(bf16), "tp", scatter_dimension=2, tiled=True)
    returned = lax.all_to_all(summed, "sp", split_axis=1, concat_axis=0, tiled=True)
    moe_grad = lax.dot_general(
        picks, returned.reshape(slots, quarter), (((0,), (0,)), ((), ())),
        preferred_element_type=f32,
    )
    mix_part = (part_cot.astype(f32) + moe_grad).astype(bf16)
    mix_grad = lax.all_gather(mix_part, "tp", axis=1, tiled=True)
    out_grad = lax.dot_general(
        mix_grad, out_proj, (((1,), (1,)), ((), ())), preferred_element_type=f32
    ).astype(bf16)
    span_part = mixer_span(queries, out_grad, cum)
    far = lax.all_gather(span_part, "sp")
    mix_cols = lax.all_to_all(mix_grad, "sp", split_axis=1, concat_axis=0, tiled=True)
    grad_outproj = lax.dot_general(
        mix_cols, all_mixer, (((0,), (0,)), ((), ())), preferred_element_type=f32
    )
    me = lax.axis_index("sp").astype(jnp.int32).reshape(1)
    grad_queries, grad_keys, grad_values, grad_decay = mixer_main(
        me, queries, key_rows, values, out_grad, cum, states, far
    )
    return (
        grad_gate,
        grad_up,
        grad_down,
        grad_outproj,
        grad_queries,
        grad_keys,
        grad_values,
        grad_decay,
    )


def solution(mesh):
    placed = (
        P("sp", None),
        P("sp", None),
        P("sp", None),
        P("sp", None),
        P("sp", None, "tp"),
        P("sp", None, "tp"),
        P("sp", "tp", None),
        P("tp", None),
        P("sp", "tp"),
        P("sp", "tp"),
        P("sp", "tp"),
        P("sp", "tp"),
        P("sp", "tp"),
        P("sp", "tp", None, None),
    )
    return jax.shard_map(
        body,
        mesh=mesh,
        in_specs=placed,
        out_specs=(
            P("sp", None, "tp"),
            P("sp", None, "tp"),
            P("sp", "tp", None),
            P("sp", "tp"),
            P("sp", "tp"),
            P("sp", "tp"),
            P("sp", "tp"),
            P("sp", "tp"),
        ),
        check_vma=False,
    )
```

time: 832 us -> 450 us (0.54)
  local copies, waits for them, and re-layouts: 255 us -> 18 us
  other arithmetic: 221 us -> 12.2 us
  waiting for transfers between devices: 144 us -> 237 us
  matrix products: 100 us -> 48.9 us
  Pallas kernels: 0 us -> 18.8 us
  blocking collectives: 71.1 us -> 86.5 us
    while x59 -> x0, local copies, waits for them, and re-layouts: 167 us -> none
    all_gather x1 -> x2, waiting for transfers between devices: 0.02 us -> 105 us  [the longest x1 66.5 us: body(): all_mixer = lax.all_gather(mixer_out, 'sp', axis=0, tiled=True)]
    dot_general x12 -> x0, other arithmetic: 102 us -> none  [the longest x4 40 us: block_grads(): jnp.einsum('hts,htd,htsd->hsd', couplings, queries, decays, precision=hig...]
    select_n x8 -> x0, other arithmetic: 53 us -> none  [the longest x4 50.1 us: block_grads(): jnp.where(causal_mask, jnp.exp(jnp.where(causal_mask, log_gaps, 0.0)), 0.0)]
    dot_general x37 -> x11, matrix products: 89.4 us -> 37.2 us  [the longest x1 5.68 us: body(): jnp.einsum('erd,efd->erf', got_cot, down_proj, preferred_element_type=f32)]
    all_to_all x0 -> x1, blocking collectives: none -> 41.5 us  [body(): lax.all_to_all(summed, 'sp', split_axis=1, concat_axis=0, tiled=True)]
    all_to_all x1, waiting for transfers between devices: 31.4 us -> 0.01 us  [body(): lax.all_to_all(mix_grad, 'sp', split_axis=1, concat_axis=0, tiled=True)]
    another operation x4 -> x0, other arithmetic: 27.3 us -> none  [the longest x1 26.1 us: body(): cumulative = jnp.cumsum(to_blocks(log_decay, KEY_CHANNELS), axis=2)]
  transfers between devices with their start and end apart: 8 -> 8, of which waited for: 5 -> 7; matrix products, arithmetic and copies ran while one was open for 60% -> 7% of each run, Pallas kernels for 0% -> 2%
where the time goes in v1:
time: 450 us; the launch traced here: 449 us
  waiting for transfers between devices  237 us (53%)
  blocking collectives  86.5 us (19%)
  matrix products  48.9 us (11%)
  Pallas kernels  18.8 us (4%)
  local copies, waits for them, and re-layouts  18 us (4%)
  between operations  14.3 us (3%)
  starting transfers between devices  13.6 us (3%)
  other arithmetic  12.2 us (3%)
    all_gather x1, waiting for transfers between devices, body(): all_mixer = lax.all_gather(mixer_out, 'sp', axis=0, tiled=True)  66.5 us
    all_to_all x1, blocking collectives, body(): lax.all_to_all(rows_cot, 'sp', split_axis=0, concat_axis=1, tiled=True)  44.9 us
    reduce_scatter x1, waiting for transfers between devices, body(): lax.psum_scatter(partial_value.astype(bf16), 'tp', scatter_dimension=2, t...  43.4 us
    all_to_all x1, blocking collectives, body(): lax.all_to_all(summed, 'sp', split_axis=1, concat_axis=0, tiled=True)  41.5 us
    all_gather x1, waiting for transfers between devices, body(): lax.all_gather(got_cot, 'tp', axis=2, tiled=True)  38.5 us
    all_gather x1, waiting for transfers between devices, body(): far = lax.all_gather(span_part, 'sp')  38.2 us
    all_to_all x1, waiting for transfers between devices, body(): lax.all_to_all(rows_in, 'sp', split_axis=0, concat_axis=1, tiled=True)  31.5 us
    all_gather x1, waiting for transfers between devices, body(): mix_grad = lax.all_gather(mix_part, 'tp', axis=1, tiled=True)  15.3 us
  transfers between devices with their start and end apart: 8, of which 7 were waited for; matrix products, arithmetic and copies ran while one was open for 7% of the time, Pallas kernels for 2%

profile of v1, /device:TPU:0, one launch (start us, length us, event | category | flops | bytes accessed | tf_op | source)
XLA Modules:
  0.0 449.1 jit_solution(2125008180005482633)
XLA Ops:
  9.5 2.8 convolution_convert_fusion
  12.3 7.6 %all-to-all-start = ((bf16[16,48,1024]{2,1,0:T(8,128)(2,1)}), bf16[16,48,1024]{2,1,0:T(8,128)(2,1)}, u32[]{:S(2)}, u32[]{:S(2)}) async-start(bf16[16,48,1024]{2,1,0:T(8,128)(2,1)} %bitcast.96), calls=%async_computation | async-start | bytes 3145728 | tf_op jit(solution)/shard_map/all_to_all | solution.py:283
  20.2 31.5 %all-to-all-done = bf16[16,48,1024]{2,1,0:T(8,128)(2,1)} async-done(((bf16[16,48,1024]{2,1,0:T(8,128)(2,1)}), bf16[16,48,1024]{2,1,0:T(8,128)(2,1)}, u32[]{:S(2)}, u32[]{:S(2)}) %all-to-all-start) | async-done | bytes 1572896 | tf_op jit(solution)/shard_map/all_to_all | solution.py:283
  51.8 1.6 multiply_convert_fusion
  53.5 44.9 %all_to_all.52 = bf16[16,48,1024]{2,1,0:T(8,128)(2,1)} all-to-all(bf16[16,48,1024]{2,1,0:T(8,128)(2,1)S(1)} %bitcast.98), channel_id=1, replica_groups=mesh['sp'=16,'tp'=2] {'sp'}, dimensions={0} | all-to-all | bytes 3145728 | tf_op jit(solution)/shard_map/all_to_all | solution.py:284
  98.5 2.9 all-gather.7.cloned.1.call-done
  101.3 5.0 %fusion.8 = f32[768,512]{1,0:T(8,128)} fusion(bf16[1,768,2048]{2,1,0:T(8,128)(2,1)} %all-gather.7.cloned.1.call-done, bf16[1,2048,512]{2,1,0:T(8,128)(2,1)S(1)} %copy-done), kind=kOutput, calls=%fused_computation.9 | convolution fusion | flops 1610612736 | bytes 6815744 | tf_op jit(solution)/shard_map/erd,edf->erf/dot_general | solution.py:294
  106.3 3.0 fusion.10
  109.3 38.5 %all-gather.9.cloned.1.call-done = bf16[1,768,2048]{2,1,0:T(8,128)(2,1)} async-done(((bf16[1,768,1024]{2,1,0:T(8,128)(2,1)}), bf16[1,768,2048]{2,1,0:T(8,128)(2,1)}) %all-gather.9.cloned.1.call-update) | async-done | bytes 3145744 | tf_op jit(solution)/shard_map/all_gather | solution.py:288
  147.8 5.7 %multiply_convert_fusion.2 = (bf16[768,512]{1,0:T(8,128)(2,1)S(1)}, bf16[768,512]{1,0:T(8,128)(2,1)S(1)}) fusion(f32[768,512]{1,0:T(8,128)} %fusion.8, f32[768,512]{1,0:T(8,128)} %fusion.10, bf16[1,512,2048]{2,1,0:T(8,128)(2,1)} %param.20, bf16[1,768,2048]{2,1,0:T(8,128)(2,1)} %all-gather.9.cloned.1.call-done), kind=kOutput, calls=%fused_computation.32 | convolution fusion | flops 1615724544 | bytes 9961472 | tf_op jit(solution)/shard_map/erd,efd->erf/dot_general | solution.py:298
  153.5 1.8 fusion.31
  155.4 3.5 fusion.12
  159.1 43.4 %reduce-scatter.2.cloned.1.call-done = bf16[1,768,1024]{2,1,0:T(8,128)(2,1)} async-done(((bf16[1,768,2048]{2,1,0:T(8,128)(2,1)}), bf16[1,768,1024]{2,1,0:T(8,128)(2,1)}) %reduce-scatter.2.cloned.1.call-update) | async-done | bytes 1572880 | tf_op jit(solution)/shard_map/reduce_scatter | solution.py:315
  202.5 5.5 %copy.68 = bf16[1,768,1024]{2,0,1:T(2,128)(2,1)} copy(bf16[1,768,1024]{2,1,0:T(8,128)(2,1)} %reduce-scatter.2.cloned.1.call-done) | data formatting | bytes 3145728 | tf_op jit(solution)/shard_map/reduce_scatter | solution.py:315
  208.4 11.2 %reduce = bf16[768,1024]{1,0:T(8,128)(2,1)S(1)} reduce(bf16[768,1,1024]{2,1,0:T(2,128)(2,1)} %bitcast.93, bf16[]{:T(256)} %broadcast.15), dimensions={1}, to_apply=%bitcast.92.reduce_sub_computation | reduce | bytes 3145730
  219.7 2.3 reshape.130
  222.0 41.5 %all_to_all.53 = bf16[16,2,24576]{2,1,0:T(2,128)(2,1)S(1)} all-to-all(bf16[16,2,24576]{2,1,0:T(2,128)(2,1)} %reshape.130), channel_id=1, replica_groups=mesh['sp'=16,'tp'=2] {'sp'}, dimensions={0} | all-to-all | bytes 3145728 | tf_op jit(solution)/shard_map/all_to_all | solution.py:316
  263.5 6.3 %reshape.131 = bf16[768,1,1024]{2,1,0:T(2,128)(2,1)} reshape(bf16[16,2,24576]{2,1,0:T(2,128)(2,1)S(1)} %all_to_all.53) | data formatting | bytes 3145728
  269.8 3.5 fusion.43
  274.8 4.2 mixer_pre.1
  279.0 15.3 %all-gather.11.cloned.1.call-done = bf16[256,2048]{1,0:T(8,128)(2,1)} async-done(((bf16[256,1024]{1,0:T(8,128)(2,1)}), bf16[256,2048]{1,0:T(8,128)(2,1)}) %all-gather.11.cloned.1.call-update) | async-done | bytes 1048592 | tf_op jit(solution)/shard_map/all_gather | solution.py:322
  294.3 4.6 %convolution_convert_fusion.1.g_ref = bf16[256,1024]{1,0:T(8,128)(2,1)} fusion(bf16[256,2048]{1,0:T(8,128)(2,1)} %all-gather.11.cloned.1.call-done, bf16[1024,2048]{1,0:T(8,128)(2,1)} %param.21), kind=kOutput, calls=%fused_computation.37 | convolution fusion | flops 1074003968 | bytes 5767168 | tf_op jit(solution)/shard_map/dot_general | solution.py:323
  298.9 3.9 mixer_span.1
  302.8 1.3 copy_bitcast_fusion
  304.1 5.6 %all-to-all-start.3 = ((bf16[256,16,128]{2,0,1:T(8,128)(2,1)}), bf16[256,16,128]{2,0,1:T(8,128)(2,1)S(1)}, u32[]{:S(2)}, u32[]{:S(2)}) async-start(bf16[256,16,128]{2,0,1:T(8,128)(2,1)} %copy_bitcast_fusion), calls=%async_computation.4 | async-start | bytes 2097152 | tf_op jit(solution)/shard_map/all_to_all | solution.py:328
  309.7 5.2 %fusion.28 = bf16[1,2048,512]{2,1,0:T(8,128)(2,1)} fusion(bf16[768,512]{1,0:T(8,128)(2,1)S(1)} %copy-done.6, bf16[1,768,2048]{2,1,0:T(8,128)(2,1)} %all-gather.7.cloned.1.call-done), kind=kOutput, calls=%fused_computation.20 | convolution fusion | flops 1611661312 | bytes 6029312 | tf_op jit(solution)/shard_map/erd,erf->edf/dot_general | solution.py:306
  314.9 3.2 fusion.25
  318.1 3.3 fusion.22
  321.5 66.5 %all-gather.13.cloned.1.call-done = bf16[4096,1024]{1,0:T(8,128)(2,1)} async-done(((bf16[256,1024]{1,0:T(8,128)(2,1)}), bf16[4096,1024]{1,0:T(8,128)(2,1)}) %all-gather.13.cloned.1.call-update) | async-done | bytes 8388624 | tf_op jit(solution)/shard_map/all_gather | solution.py:292
  387.9 5.5 %fusion.66 = f32[128,1024]{1,0:T(8,128)} fusion(bf16[4096,128]{1,0:T(8,128)(2,1)S(1)} %bitcast.94, bf16[4096,1024]{1,0:T(8,128)(2,1)} %all-gather.13.cloned.1.call-done), kind=kOutput, calls=%fused_computation.65 | convolution fusion | flops 1073741824 | bytes 9961472 | tf_op jit(solution)/shard_map/dot_general | solution.py:329
  393.4 38.2 %all-gather.15.cloned.1.call-done = f32[1152,512]{1,0:T(8,128)} async-done(((f32[72,512]{1,0:T(8,128)}), f32[1152,512]{1,0:T(8,128)}) %all-gather.15.cloned.1.call-update) | async-done | bytes 2359312 | tf_op jit(solution)/shard_map/all_gather | solution.py:327
  431.6 10.6 %mixer_main.1 = (bf16[256,512]{1,0:T(8,128)(2,1)}, bf16[256,512]{1,0:T(8,128)(2,1)}, bf16[256,1024]{1,0:T(8,128)(2,1)}, f32[256,512]{1,0:T(8,128)}) custom-call(s32[1]{0:T(128)} %bitcast.19.me_ref, bf16[256,512]{1,0:T(8,128)(2,1)} %q_ref.3, bf16[256,512]{1,0:T(8,128)(2,1)} %k_ref.3, bf16[256,1024]{1,0:T(8,128)(2,1)} %v_ref.3, ...), custom_call_target="tpu_custom_call" | custom-call | flops 4000000000 | bytes 6000000 | tf_op jit(solution)/shard_map/mixer_main/pallas_call | solution.py:196
  (54 shorter events, 5.0 us)
Async XLA Ops:
  7.2 94.2 %copy-start = (bf16[1,2048,512]{2,1,0:T(8,128)(2,1)S(1)}, bf16[1,2048,512]{2,1,0:T(8,128)(2,1)}, u32[]{:S(2)}) copy-start(bf16[1,2048,512]{2,1,0:T(8,128)(2,1)} %param.18) | copy-start | bytes 6291460
  12.3 7.6 %copy-start.8 = (f32[256,2]{0,1:T(2,128)S(1)}, f32[256,2]{0,1:T(2,128)}, u32[]{:S(2)}) copy-start(f32[256,2]{0,1:T(2,128)} %param.17) | copy-start | bytes 6148
  12.3 39.5 %all-to-all-start = ((bf16[16,48,1024]{2,1,0:T(8,128)(2,1)}), bf16[16,48,1024]{2,1,0:T(8,128)(2,1)}, u32[]{:S(2)}, u32[]{:S(2)}) async-start(bf16[16,48,1024]{2,1,0:T(8,128)(2,1)} %bitcast.96), calls=%async_computation | async-start | bytes 3145728 | tf_op jit(solution)/shard_map/all_to_all | solution.py:283
  19.9 81.5 %all-gather.7.cloned.1.call-start = ((), (), s32[]{:S(2)}) async-start(), calls=%async_computation.5 | async-start | bytes 4718592 | tf_op jit(solution)/shard_map/all_gather | solution.py:287
  51.8 96.0 %all-gather.9.cloned.1.call-start = ((), (), s32[]{:S(2)}) async-start(), calls=%async_computation.6 | async-start | bytes 4718592 | tf_op jit(solution)/shard_map/all_gather | solution.py:288
  98.4 104.0 %reduce-scatter.2.cloned.1.call-start = ((), (), s32[]{:S(2)}) async-start(), calls=%async_computation.7 | async-start | bytes 4718592 | tf_op jit(solution)/shard_map/reduce_scatter | solution.py:315
  101.3 5.0 %copy-start.2 = (bf16[1,2048,512]{2,1,0:T(8,128)(2,1)S(1)}, bf16[1,2048,512]{2,1,0:T(8,128)(2,1)}, u32[]{:S(2)}) copy-start(bf16[1,2048,512]{2,1,0:T(8,128)(2,1)} %param.19) | copy-start | bytes 6291460
  101.3 5.0 %copy-start.9 = (bf16[1,768,2048]{2,1,0:T(8,128)(2,1)S(1)}, bf16[1,768,2048]{2,1,0:T(8,128)(2,1)}, u32[]{:S(2)}) copy-start(bf16[1,768,2048]{2,1,0:T(8,128)(2,1)} %all-gather.7.cloned.1.call-done) | copy-start | bytes 9437188
  153.5 1.9 copy-start.5
  153.5 1.9 copy-start.3
  158.9 135.4 %all-gather.11.cloned.1.call-start = ((), (), s32[]{:S(2)}) async-start(), calls=%async_computation.8 | async-start | bytes 1572864 | tf_op jit(solution)/shard_map/all_gather | solution.py:322
  269.8 4.2 copy-start.7
  273.3 114.6 %all-gather.13.cloned.1.call-start = ((), (), s32[]{:S(2)}) async-start(), calls=%async_computation.9 | async-start | bytes 8912896 | tf_op jit(solution)/shard_map/all_gather | solution.py:292
  273.9 157.6 %all-gather.15.cloned.1.call-start = ((), (), s32[]{:S(2)}) async-start(), calls=%async_computation.10 | async-start | bytes 2506752 | tf_op jit(solution)/shard_map/all_gather | solution.py:327
  298.9 3.9 copy-start.4
  302.8 6.9 %copy-start.6 = (bf16[768,512]{1,0:T(8,128)(2,1)S(1)}, bf16[768,512]{1,0:T(8,128)(2,1)}, u32[]{:S(2)}) copy-start(bf16[768,512]{1,0:T(8,128)(2,1)} %copy-done.5) | copy-start | bytes 2359300
  304.1 83.9 %all-to-all-start.3 = ((bf16[256,16,128]{2,0,1:T(8,128)(2,1)}), bf16[256,16,128]{2,0,1:T(8,128)(2,1)S(1)}, u32[]{:S(2)}, u32[]{:S(2)}) async-start(bf16[256,16,128]{2,0,1:T(8,128)(2,1)} %copy_bitcast_fusion), calls=%async_computation.4 | async-start | bytes 2097152 | tf_op jit(solution)/shard_map/all_to_all | solution.py:328
  309.7 5.2 %copy-start.10 = (bf16[1,768,2048]{2,1,0:T(8,128)(2,1)S(1)}, bf16[1,768,2048]{2,1,0:T(8,128)(2,1)}, u32[]{:S(2)}) copy-start(bf16[1,768,2048]{2,1,0:T(8,128)(2,1)} %all-gather.7.cloned.1.call-done) | copy-start | bytes 9437188
  314.9 3.2 copy-start.11
  314.9 3.2 copy-start.12
  314.9 3.2 copy-start.13
  431.6 10.7 %copy-start.1 = (bf16[1,2048,512]{2,1,0:T(8,128)(2,1)S(1)}, bf16[1,2048,512]{2,1,0:T(8,128)(2,1)}, u32[]{:S(2)}) copy-start(bf16[1,2048,512]{2,1,0:T(8,128)(2,1)} %param.18) | copy-start | bytes 6291460
Sparse Core Ops, SparseCore 0:
  51.9 49.3 all-gather.6
  102.9 44.8 all-gather.8
  159.0 43.4 reduce-scatter.1
  273.5 20.7 all-gather.10
  296.3 91.5 all-gather.12
  390.6 40.8 all-gather.14

commit v2 on v1

--- a/solution.py
+++ b/solution.py
@@ -223,6 +223,80 @@
     )(me, queries, key_rows, values, out_grad, cum, states, far)
 
 
+def exchange_kernel(axis, gather, count, *refs):
+    ins, outs = refs[:count], refs[count : 2 * count]
+    send, recv, own = refs[2 * count :]
+    n = outs[0].shape[0]
+    me = lax.axis_index(axis)
+    barrier = pltpu.get_barrier_semaphore()
+
+    def greet(o, _):
+        pl.semaphore_signal(
+            barrier, 1, device_id={axis: lax.rem(me + o, n)}, device_id_type=pl.DeviceIdType.MESH
+        )
+        return _
+
+    lax.fori_loop(1, n, greet, 0)
+    pl.semaphore_wait(barrier, n - 1)
+
+    def copy(c, o):
+        peer = lax.rem(me + o, n)
+        return pltpu.make_async_remote_copy(
+            src_ref=ins[c] if gather else ins[c].at[peer],
+            dst_ref=outs[c].at[me],
+            send_sem=send.at[c, o],
+            recv_sem=recv.at[c, o],
+            device_id={axis: peer},
+            device_id_type=pl.DeviceIdType.MESH,
+        )
+
+    for c in range(count):
+
+        def start(o, _, c=c):
+            copy(c, o).start()
+            return _
+
+        lax.fori_loop(1, n, start, 0)
+    locals_ = [
+        pltpu.make_async_copy(ins[c] if gather else ins[c].at[me], outs[c].at[me], own.at[c])
+        for c in range(count)
+    ]
+    for one in locals_:
+        one.start()
+    for one in locals_:
+        one.wait()
+    for c in range(count):
+
+        def finish(o, _, c=c):
+            copy(c, o).wait()
+            return _
+
+        lax.fori_loop(1, n, finish, 0)
+
+
+def exchange(arrays, axis, gather, ident, name):
+    n = lax.axis_size(axis)
+    count = len(arrays)
+    shapes = [((n,) + a.shape) if gather else a.shape for a in arrays]
+    size = sum(a.size for a in arrays) * (n if gather else 1)
+    return pl.pallas_call(
+        functools.partial(exchange_kernel, axis, gather, count),
+        in_specs=[pl.BlockSpec(memory_space=pl.ANY)] * count,
+        out_specs=[pl.BlockSpec(memory_space=pl.ANY)] * count,
+        out_shape=[jax.ShapeDtypeStruct(s, a.dtype) for s, a in zip(shapes, arrays)],
+        scratch_shapes=[
+            pltpu.SemaphoreType.DMA((count, n)),
+            pltpu.SemaphoreType.DMA((count, n)),
+            pltpu.SemaphoreType.DMA((count,)),
+        ],
+        compiler_params=pltpu.CompilerParams(collective_id=ident, has_side_effects=True),
+        cost_estimate=pl.CostEstimate(
+            flops=0, bytes_accessed=40 * 2 * size, transcendentals=0
+        ),
+        name=name,
+    )(*arrays)
+
+
 def dispatch_places(routes, experts, capacity):
     tok, top = routes.shape
     flat = routes.reshape(-1)
@@ -234,6 +308,15 @@
     )
     ranks = jnp.sum(jnp.where(onehot, before, 0.0), axis=1).astype(jnp.int32)
     return (flat * capacity + ranks).reshape(tok, top)
+
+
+def to_expert_rows(a, local_experts, capacity):
+    sources, _, width = a.shape
+    return (
+        a.reshape(sources, local_experts, capacity, width)
+        .transpose(1, 0, 2, 3)
+        .reshape(local_experts, sources * capacity, width)
+    )
 
 
 def body(
@@ -253,15 +336,12 @@
     saved_state,
 ):
     sp_count = lax.axis_size("sp")
-    tp_count = lax.axis_size("tp")
     local_experts = gate_proj.shape[0]
     experts = local_experts * sp_count
     tok_local, model_width = layer_cot.shape
     top_count = routes.shape[1]
     capacity = 3 * tok_local // experts
     slots = experts * capacity
-    quarter = model_width // tp_count
-    tp_rank = lax.axis_index("tp")
 
     places = dispatch_places(routes, experts, capacity)
     slot_ids = jnp.arange(slots, dtype=jnp.int32)
@@ -271,22 +351,13 @@
         jnp.sum(jnp.where(hits[j], route_weights[None, :, j], 0.0), axis=1)
         for j in range(top_count)
     )
-    part_in = lax.dynamic_slice_in_dim(moe_input, tp_rank * quarter, quarter, 1)
-    part_cot = lax.dynamic_slice_in_dim(layer_cot, tp_rank * quarter, quarter, 1)
-    rows_in = jnp.dot(picks, part_in, preferred_element_type=f32).astype(bf16)
+    rows_in = jnp.dot(picks, moe_input, preferred_element_type=f32).astype(bf16)
     rows_cot = (
-        slot_weights[:, None] * jnp.dot(picks, part_cot, preferred_element_type=f32)
+        slot_weights[:, None] * jnp.dot(picks, layer_cot, preferred_element_type=f32)
     ).astype(bf16)
-    rows_in = rows_in.reshape(experts, capacity, quarter)
-    rows_cot = rows_cot.reshape(experts, capacity, quarter)
-    got_in, got_cot = (
-        lax.all_to_all(rows_in, "sp", split_axis=0, concat_axis=1, tiled=True),
-        lax.all_to_all(rows_cot, "sp", split_axis=0, concat_axis=1, tiled=True),
-    )
-    got_in, got_cot = (
-        lax.all_gather(got_in, "tp", axis=2, tiled=True),
-        lax.all_gather(got_cot, "tp", axis=2, tiled=True),
-    )
+    split = (experts // local_experts, local_experts * capacity, model_width)
+    got = exchange([rows_in.reshape(split), rows_cot.reshape(split)], "sp", False, 0, "to_experts")
+    got_in, got_cot = (to_expert_rows(a, local_experts, capacity) for a in got)
     saved = saved_state[0].transpose(2, 0, 1).reshape(DV, -1)
     cum, states = mixer_pre(key_rows, values, log_decay, saved)
     all_mixer = lax.all_gather(mixer_out, "sp", axis=0, tiled=True)
@@ -312,14 +383,20 @@
     partial_value = jnp.einsum(
         "erf,edf->erd", grad_pre_gate, gate_proj, preferred_element_type=f32
     ) + jnp.einsum("erf,edf->erd", grad_pre_up, up_proj, preferred_element_type=f32)
-    summed = lax.psum_scatter(partial_value.astype(bf16), "tp", scatter_dimension=2, tiled=True)
-    returned = lax.all_to_all(summed, "sp", split_axis=1, concat_axis=0, tiled=True)
-    moe_grad = lax.dot_general(
-        picks, returned.reshape(slots, quarter), (((0,), (0,)), ((), ())),
+    back = (
+        partial_value.astype(bf16)
+        .reshape(local_experts, sp_count, capacity, model_width)
+        .transpose(1, 0, 2, 3)
+        .reshape(split)
+    )
+    back, all_mixer = lax.optimization_barrier((back, all_mixer))
+    (returned,) = exchange([back], "sp", False, 1, "to_tokens")
+    moe_part = lax.dot_general(
+        picks, returned.reshape(slots, model_width), (((0,), (0,)), ((), ())),
         preferred_element_type=f32,
-    )
-    mix_part = (part_cot.astype(f32) + moe_grad).astype(bf16)
-    mix_grad = lax.all_gather(mix_part, "tp", axis=1, tiled=True)
+    ).astype(bf16)
+    (moe_parts,) = exchange([moe_part], "tp", True, 2, "tp_parts")
+    mix_grad = (layer_cot.astype(f32) + jnp.sum(moe_parts.astype(f32), axis=0)).astype(bf16)
     out_grad = lax.dot_general(
         mix_grad, out_proj, (((1,), (1,)), ((), ())), preferred_element_type=f32
     ).astype(bf16)

time: 450 us -> 419 us (0.931)
  Pallas kernels: 18.8 us -> 299 us
  waiting for transfers between devices: 237 us -> 28.4 us
  blocking collectives: 86.5 us -> 0 us
  local copies, waits for them, and re-layouts: 18 us -> 9.44 us
  other arithmetic: 12.2 us -> 3.69 us
  starting transfers between devices: 13.6 us -> 21.7 us
  matrix products: 48.9 us -> 41.9 us
    pallas_call x0 -> x3, Pallas kernels: none -> 281 us  [exchange(): pl.pallas_call(functools.partial(exchange_kernel, axis, gather, count), i...]
    all_to_all x2 -> x0, blocking collectives: 86.5 us -> none  [the longest x1 44.9 us: body(): lax.all_to_all(rows_cot, 'sp', split_axis=0, concat_axis=1, tiled=True)]
    all_gather x1, waiting for transfers between devices: 66.5 us -> 0.01 us  [body(): all_mixer = lax.all_gather(mixer_out, 'sp', axis=0, tiled=True)]
    all_gather x3 -> x0, waiting for transfers between devices: 56.7 us -> none  [the longest x1 38.5 us: body(): lax.all_gather(got_cot, 'tp', axis=2, tiled=True)]
    reduce_scatter x1 -> x0, waiting for transfers between devices: 43.4 us -> none  [body(): lax.psum_scatter(partial_value.astype(bf16), 'tp', scatter_dimension=2, t...]
    all_to_all x1 -> x0, waiting for transfers between devices: 31.5 us -> none  [body(): lax.all_to_all(rows_in, 'sp', split_axis=0, concat_axis=1, tiled=True)]
    all_gather x1, waiting for transfers between devices: 38.2 us -> 12 us  [body(): far = lax.all_gather(span_part, 'sp')]
    all_to_all x1, starting transfers between devices: 5.62 us -> 21.6 us  [body(): lax.all_to_all(mix_grad, 'sp', split_axis=1, concat_axis=0, tiled=True)]
  transfers between devices with their start and end apart: 8 -> 3, of which waited for: 7 -> 2; matrix products, arithmetic and copies ran while one was open for 7% -> 10% of each run, Pallas kernels for 2% -> 40%
where the time goes in v2:
time: 419 us
  Pallas kernels  299 us (71%)
  matrix products  41.9 us (10%)
  waiting for transfers between devices  28.4 us (7%)
  starting transfers between devices  21.7 us (5%)
  between operations  14.4 us (3%)
  local copies, waits for them, and re-layouts  9.44 us (2%)
    pallas_call x3, Pallas kernels, exchange(): pl.pallas_call(functools.partial(exchange_kernel, axis, gather, count), i...  281 us
    all_to_all x1, starting transfers between devices, body(): lax.all_to_all(mix_grad, 'sp', split_axis=1, concat_axis=0, tiled=True)  21.6 us
    all_to_all x1, waiting for transfers between devices, body(): lax.all_to_all(mix_grad, 'sp', split_axis=1, concat_axis=0, tiled=True)  15.7 us
    all_gather x1, waiting for transfers between devices, body(): far = lax.all_gather(span_part, 'sp')  12 us
    pallas_call x1, Pallas kernels, mixer_main(): pl.pallas_call(main_kernel, grid_spec=pltpu.PrefetchScalarGridSpec(num_sc...  10.6 us
  transfers between devices with their start and end apart: 3, of which 2 were waited for; matrix products, arithmetic and copies ran while one was open for 10% of the time, Pallas kernels for 40%

profile of v2, /device:TPU:0, one launch (start us, length us, event | category | flops | bytes accessed | tf_op | source)
XLA Modules:
  0.0 418.9 jit_solution(7585956014472330329)
XLA Ops:
  7.2 0.7 all-gather.4.cloned.1.call-update
  8.0 0.8 copy.45
  9.5 1.7 copy.49.s_ref
  11.2 0.7 multiply_add_fusion
  11.9 0.8 fusion.26
  13.0 2.6 convolution_convert_fusion
  15.6 2.6 multiply_convert_fusion
  18.2 164.4 %to_experts.1 = (bf16[16,48,2048]{2,1,0:T(8,128)(2,1)}, bf16[16,48,2048]{2,1,0:T(8,128)(2,1)}) custom-call(bf16[16,48,2048]{2,1,0:T(8,128)(2,1)} %bitcast.58, bf16[16,48,2048]{2,1,0:T(8,128)(2,1)} %bitcast.62), custom_call_target="tpu_custom_call" | custom-call | bytes 251658240 | tf_op jit(solution)/shard_map/to_experts/pallas_call | solution.py:282
  182.6 4.3 %mixer_pre.1 = (f32[256,512]{1,0:T(8,128)}, f32[5,64,512]{2,1,0:T(8,128)}) custom-call(bf16[256,512]{1,0:T(8,128)(2,1)} %k_ref.3, bf16[256,1024]{1,0:T(8,128)(2,1)} %v_ref.3, f32[256,512]{1,0:T(8,128)} %ld_ref.1, f32[64,512]{1,0:T(8,128)} %copy.49.s_ref), custom_call_target="tpu_custom_call" | custom-call | flops 1000000000 | bytes 4000000 | tf_op jit(solution)/shard_map/mixer_pre/pallas_call | solution.py:163
  187.0 3.8 fusion.5
  190.8 1.8 fusion.8
  193.3 1.2 copy-done.13
  194.5 2.3 multiply_convert_fusion.2
  196.8 1.8 fusion.3
  198.7 3.5 add_convert_fusion
  202.1 81.9 %to_tokens.1 = bf16[16,48,2048]{2,1,0:T(8,128)(2,1)} custom-call(bf16[16,48,2048]{2,1,0:T(8,128)(2,1)} %bitcast.59), custom_call_target="tpu_custom_call" | custom-call | bytes 125829120 | tf_op jit(solution)/shard_map/to_tokens/pallas_call | solution.py:282
  284.0 3.9 convolution_convert_fusion.4.refs_0_
  287.9 34.4 %tp_parts.1 = bf16[2,256,2048]{2,1,0:T(8,128)(2,1)} custom-call(bf16[256,2048]{1,0:T(8,128)(2,1)} %convolution_convert_fusion.4.refs_0_), custom_call_target="tpu_custom_call" | custom-call | bytes 83886080 | tf_op jit(solution)/shard_map/tp_parts/pallas_call | solution.py:282
  322.3 2.4 convert_reduce_fusion
  325.0 1.8 copy-done.8
  326.9 2.1 convolution_convert_fusion.5.g_ref
  328.9 3.8 mixer_span.1
  332.8 1.3 copy.47
  334.1 21.6 %all-to-all-start = ((bf16[256,16,128]{0,2,1:T(8,128)(2,1)}), bf16[256,16,128]{0,2,1:T(8,128)(2,1)S(1)}, u32[]{:S(2)}, u32[]{:S(2)}) async-start(bf16[256,16,128]{0,2,1:T(8,128)(2,1)} %bitcast.16), calls=%async_computation | async-start | bytes 2097152 | tf_op jit(solution)/shard_map/all_to_all | solution.py:405
  355.8 5.3 %fusion = bf16[1,2048,512]{2,1,0:T(8,128)(2,1)} fusion(bf16[768,2048]{1,0:T(8,128)(2,1)} %bitcast.78, bf16[768,512]{1,0:T(8,128)(2,1)S(1)} %copy-done.7), kind=kOutput, calls=%fused_computation.7 | convolution fusion | flops 1611661312 | bytes 6029312 | tf_op jit(solution)/shard_map/erd,erf->edf/dot_general | solution.py:377
  361.0 3.2 fusion.1
  364.2 3.3 fusion.2
  367.6 15.7 %all-to-all-done = bf16[256,16,128]{0,2,1:T(8,128)(2,1)S(1)} async-done(((bf16[256,16,128]{0,2,1:T(8,128)(2,1)}), bf16[256,16,128]{0,2,1:T(8,128)(2,1)S(1)}, u32[]{:S(2)}, u32[]{:S(2)}) %all-to-all-start) | async-done | bytes 1048608 | tf_op jit(solution)/shard_map/all_to_all | solution.py:405
  383.3 0.7 copy.48
  384.0 5.5 %fusion.28 = f32[128,1024]{1,0:T(8,128)} fusion(bf16[4096,128]{1,0:T(8,128)(2,1)S(1)} %bitcast.60, bf16[4096,1024]{1,0:T(8,128)(2,1)} %all-gather.4.cloned.1.call-done), kind=kOutput, calls=%fused_computation.47 | convolution fusion | flops 1073741824 | bytes 9961472 | tf_op jit(solution)/shard_map/dot_general | solution.py:406
  389.4 12.0 %all-gather.6.cloned.1.call-done = f32[1152,512]{1,0:T(8,128)} async-done(((f32[72,512]{1,0:T(8,128)}), f32[1152,512]{1,0:T(8,128)}) %all-gather.6.cloned.1.call-update) | async-done | bytes 2359312 | tf_op jit(solution)/shard_map/all_gather | solution.py:404
  401.4 10.6 %mixer_main.1 = (bf16[256,512]{1,0:T(8,128)(2,1)}, bf16[256,512]{1,0:T(8,128)(2,1)}, bf16[256,1024]{1,0:T(8,128)(2,1)}, f32[256,512]{1,0:T(8,128)}) custom-call(s32[1]{0:T(128)} %bitcast.19.me_ref, bf16[256,512]{1,0:T(8,128)(2,1)} %q_ref.3, bf16[256,512]{1,0:T(8,128)(2,1)} %k_ref.3, bf16[256,1024]{1,0:T(8,128)(2,1)} %v_ref.3, ...), custom_call_target="tpu_custom_call" | custom-call | flops 4000000000 | bytes 6000000 | tf_op jit(solution)/shard_map/mixer_main/pallas_call | solution.py:196
  (47 shorter events, 2.1 us)
Async XLA Ops:
  7.2 179.8 %copy-start = (bf16[1,2048,512]{2,1,0:T(8,128)(2,1)S(1)}, bf16[1,2048,512]{2,1,0:T(8,128)(2,1)}, u32[]{:S(2)}) copy-start(bf16[1,2048,512]{2,1,0:T(8,128)(2,1)} %param.18) | copy-start | bytes 6291460
  7.2 5.8 %copy-start.3 = (bf16[256,2048]{1,0:T(8,128)(2,1)S(1)}, bf16[256,2048]{1,0:T(8,128)(2,1)}, u32[]{:S(2)}) copy-start(bf16[256,2048]{1,0:T(8,128)(2,1)} %param.15) | copy-start | bytes 3145732
  7.2 194.9 %all-gather.4.cloned.1.call-start = ((), (), s32[]{:S(2)}) async-start(), calls=%async_computation.1 | async-start | bytes 8912896 | tf_op jit(solution)/shard_map/all_gather | solution.py:363
  7.9 393.5 %all-gather.6.cloned.1.call-start = ((), (), s32[]{:S(2)}) async-start(), calls=%async_computation.2 | async-start | bytes 2506752 | tf_op jit(solution)/shard_map/all_gather | solution.py:404
  13.0 2.6 copy-start.4
  186.9 3.8 copy-start.2
  186.9 3.8 copy-start.11
  190.8 1.8 copy-start.14
  190.8 2.5 copy-start.9
  190.8 3.7 copy-start.13
  192.6 4.2 copy-start.16
  196.8 1.8 copy-start.6
  322.3 2.4 copy-start.5
  324.7 2.2 copy-start.8
  332.8 23.0 %copy-start.7 = (bf16[768,512]{1,0:T(8,128)(2,1)S(1)}, bf16[768,512]{1,0:T(8,128)(2,1)}, u32[]{:S(2)}) copy-start(bf16[768,512]{1,0:T(8,128)(2,1)} %copy-done.6) | copy-start | bytes 2359300
  334.1 49.2 %all-to-all-start = ((bf16[256,16,128]{0,2,1:T(8,128)(2,1)}), bf16[256,16,128]{0,2,1:T(8,128)(2,1)S(1)}, u32[]{:S(2)}, u32[]{:S(2)}) async-start(bf16[256,16,128]{0,2,1:T(8,128)(2,1)} %bitcast.16), calls=%async_computation | async-start | bytes 2097152 | tf_op jit(solution)/shard_map/all_to_all | solution.py:405
  355.7 5.3 %copy-start.12 = (bf16[16,48,2048]{2,1,0:T(8,128)(2,1)S(1)}, bf16[16,48,2048]{2,1,0:T(8,128)(2,1)}, u32[]{:S(2)}) copy-start(bf16[16,48,2048]{2,1,0:T(8,128)(2,1)} %get-tuple-element.18) | copy-start | bytes 9437188
  361.0 3.2 copy-start.10
  361.0 3.2 copy-start.15
  361.0 3.2 copy-start.17
  401.4 10.7 %copy-start.1 = (bf16[1,2048,512]{2,1,0:T(8,128)(2,1)S(1)}, bf16[1,2048,512]{2,1,0:T(8,128)(2,1)}, u32[]{:S(2)}) copy-start(bf16[1,2048,512]{2,1,0:T(8,128)(2,1)} %param.18) | copy-start | bytes 6291460
Sparse Core Ops, SparseCore 0:
  10.2 167.2 all-gather.3
  332.9 68.4 all-gather.5
